TPU v7x, 32 devices: a whole 2x2x4 slice. The times are simulated.
32 devices in a mesh: ep: 4 (over z), tp: 8 (over y, x, core).
Axes of the slice: x: 2, y: 2, z: 4, core: 2. Of those that a mesh axis runs over, the one named last changes fastest.
Arguments:
- tokens: bfloat16 [512, 2048], P('ep', 'tp'), may hold values from -6 to 6
- out_grad: bfloat16 [512, 2048], P('ep', 'tp'), may hold values from -6 to 6
- routes: int32 [512, 2], P('ep'), may hold values from 0 to 3, all different within a row; in each aligned block of 128 rows (0 to 127, 128 to 255, ...) at most 96 rows name the same one
- gates: float32 [512, 2], P('ep'), may hold values from 0.1 to 0.9
- gate_weight: bfloat16 [4, 2048, 5632], P('ep', None, 'tp'), may hold values from -0.125 to 0.125
- up_weight: bfloat16 [4, 2048, 5632], P('ep', None, 'tp'), may hold values from -0.125 to 0.125
- down_weight: bfloat16 [4, 5632, 2048], P('ep', 'tp'), may hold values from -0.078125 to 0.078125
Outputs:
- tokens_grad: bfloat16 [512, 2048], P('ep', 'tp')
- gates_grad: float32 [512, 2], P(('ep', 'tp'))
- gate_weight_grad: bfloat16 [4, 2048, 5632], P('ep', None, 'tp')
- up_weight_grad: bfloat16 [4, 2048, 5632], P('ep', None, 'tp')
- down_weight_grad: bfloat16 [4, 5632, 2048], P('ep', 'tp')
Inputs may be any that keep to these rules, and one draw needn't show every extreme that they name: `routes`: the 2 experts of a token differ. In each aligned block of 128 rows (the tokens of one index of ep) no expert is named by more than 96 rows, a bound that some block reaches.
All inputs are finite; a program needn't handle non-finite values.
Results may differ from a plain program's by a relative error of at most 0.029.
Values may be sent and summed in bfloat16 or wider, within the bound.
A program may use at most 64 MiB of HBM per device.

v0:
```python
import jax
import jax.numpy as jnp
from jax import lax
from jax.sharding import PartitionSpec as P


def expert_grads(rows, cotan, w_gate, w_up, w_down):
    pre_gate = jnp.dot(rows, w_gate, preferred_element_type=jnp.float32)
    pre_up = jnp.dot(rows, w_up, preferred_element_type=jnp.float32)
    activated = jax.nn.silu(pre_gate)
    hidden = (activated * pre_up).astype(jnp.bfloat16)
    hid_grad = jnp.dot(cotan, w_down.T, preferred_element_type=jnp.float32)
    sigmoid_gate = jax.nn.sigmoid(pre_gate)
    gate_part = (hid_grad * pre_up * sigmoid_gate * (1.0 + pre_gate * (1.0 - sigmoid_gate))).astype(
        jnp.bfloat16
    )
    up_part = (hid_grad * activated).astype(jnp.bfloat16)
    slot_dots = jnp.sum(hidden.astype(jnp.float32) * hid_grad, axis=1)
    down_grad = jnp.dot(hidden.T, cotan, preferred_element_type=jnp.float32).astype(jnp.bfloat16)
    gate_grad = jnp.dot(rows.T, gate_part, preferred_element_type=jnp.float32).astype(jnp.bfloat16)
    up_grad = jnp.dot(rows.T, up_part, preferred_element_type=jnp.float32).astype(jnp.bfloat16)
    return (gate_part, up_part, slot_dots, gate_grad, up_grad, down_grad)


def on_device(tokens, out_grad, routes, gates, gate_weight, up_weight, down_weight):
    tok_dev, top_k = routes.shape
    ep_size = lax.axis_size("ep")
    tp_size = lax.axis_size("tp")
    capacity = (3 * tok_dev + ep_size - 1) // ep_size
    buffer_rows = ep_size * capacity
    slice_width = tokens.shape[1]
    flat_expert = routes.reshape(-1)
    onehot = (flat_expert[:, None] == jnp.arange(ep_size, dtype=jnp.int32)[None, :]).astype(
        jnp.int32
    )
    slot_rank = jnp.sum((jnp.cumsum(onehot, axis=0) - onehot) * onehot, axis=1)
    slot_dest = flat_expert * capacity + slot_rank
    placed = jnp.arange(buffer_rows, dtype=jnp.int32)[:, None] == slot_dest[None, :]
    placed_float = placed.astype(jnp.float32)
    select = jnp.any(placed.reshape(buffer_rows, tok_dev, top_k), axis=2).astype(jnp.bfloat16)
    slot_gate = jnp.dot(placed_float, gates.reshape(-1), precision=lax.Precision.HIGHEST)
    sent_rows = jnp.dot(select, tokens, preferred_element_type=jnp.float32).astype(jnp.bfloat16)
    cotan_rows = jnp.dot(select, out_grad, preferred_element_type=jnp.float32)
    sent_cotan = (slot_gate[:, None] * cotan_rows).astype(jnp.bfloat16)
    recv_rows, recv_cotan = (
        lax.all_to_all(
            sent_rows.reshape(ep_size, capacity, slice_width),
            "ep",
            split_axis=0,
            concat_axis=0,
            tiled=True,
        ),
        lax.all_to_all(
            sent_cotan.reshape(ep_size, capacity, slice_width),
            "ep",
            split_axis=0,
            concat_axis=0,
            tiled=True,
        ),
    )
    whole_rows, whole_cotan = (
        lax.all_gather(recv_rows, "tp", axis=2, tiled=True),
        lax.all_gather(recv_cotan, "tp", axis=2, tiled=True),
    )
    model_width = whole_rows.shape[2]
    rows = whole_rows.reshape(buffer_rows, model_width)
    cotan = whole_cotan.reshape(buffer_rows, model_width)
    w_gate = gate_weight[0]
    w_up = up_weight[0]
    gate_part, up_part, slot_dots, gate_grad, up_grad, down_grad = expert_grads(
        rows, cotan, w_gate, w_up, down_weight[0]
    )
    partial_value = jnp.dot(gate_part, w_gate.T, preferred_element_type=jnp.float32)
    partial_value = (
        partial_value + jnp.dot(up_part, w_up.T, preferred_element_type=jnp.float32)
    ).astype(jnp.bfloat16)
    share = tok_dev // tp_size
    start = lax.axis_index("tp") * share
    summed = lax.psum(slot_dots, "tp")
    row_sums = lax.psum_scatter(
        partial_value.reshape(ep_size, capacity, model_width), "tp", scatter_dimension=2, tiled=True
    ).astype(jnp.float32)
    back_rows, back_dots = (
        lax.all_to_all(
            row_sums.astype(jnp.bfloat16), "ep", split_axis=0, concat_axis=0, tiled=True
        ).astype(row_sums.dtype),
        lax.all_to_all(
            summed.reshape(ep_size, capacity).astype(jnp.bfloat16),
            "ep",
            split_axis=0,
            concat_axis=0,
            tiled=True,
        ).astype(jnp.float32),
    )
    slot_rows = back_rows.reshape(buffer_rows, slice_width)[slot_dest]
    tokens_grad = jnp.sum(slot_rows.reshape(tok_dev, top_k, slice_width), axis=1).astype(
        jnp.bfloat16
    )
    token_dots = back_dots.reshape(buffer_rows)[slot_dest].reshape(tok_dev, top_k)
    own_dots = lax.dynamic_slice_in_dim(token_dots, start, share, 0)
    own_gates = lax.dynamic_slice_in_dim(gates, start, share, 0)
    gates_grad = own_dots / own_gates
    return (tokens_grad, gates_grad, gate_grad[None], up_grad[None], down_grad[None])


def solution(mesh):
    placed = (
        P("ep", "tp"),
        P("ep", "tp"),
        P("ep", None),
        P("ep", None),
        P("ep", None, "tp"),
        P("ep", None, "tp"),
        P("ep", "tp", None),
    )
    return jax.shard_map(
        on_device,
        mesh=mesh,
        in_specs=placed,
        out_specs=(
            P("ep", "tp"),
            P(("ep", "tp"), None),
            P("ep", None, "tp"),
            P("ep", None, "tp"),
            P("ep", "tp", None),
        ),
        check_vma=False,
    )
```

profile of v0, /device:TPU:0, one launch (start us, length us, event | category | flops | bytes accessed | tf_op | source)
XLA Modules:
  0.0 148.4 jit_solution(13399779016683613916)
XLA Ops:
  7.2 0.9 copy.32
  8.5 1.2 reduce-window.6
  11.0 1.0 convolution_convert_fusion.3
  12.1 13.7 %all_to_all.21 = bf16[4,96,256]{2,1,0:T(8,128)(2,1)} all-to-all(bf16[4,96,256]{2,1,0:T(8,128)(2,1)S(1)} %bitcast.70), channel_id=1, replica_groups=mesh['ep'=4,'tp'=8] {'ep'}, dimensions={0} | all-to-all | bytes 393216 | tf_op jit(solution)/shard_map/all_to_all | solution.py:46
  26.7 9.9 %all_to_all.22 = bf16[4,96,256]{2,1,0:T(8,128)(2,1)} all-to-all(bf16[4,96,256]{2,1,0:T(8,128)(2,1)S(1)} %bitcast.69), channel_id=1, replica_groups=mesh['ep'=4,'tp'=8] {'ep'}, dimensions={0} | all-to-all | bytes 393216 | tf_op jit(solution)/shard_map/all_to_all | solution.py:53
  36.6 14.2 %all-gather.5.cloned.1.call-done = bf16[4,96,2048]{2,1,0:T(8,128)(2,1)} async-done(((bf16[4,96,256]{2,1,0:T(8,128)(2,1)}), bf16[4,96,2048]{2,1,0:T(8,128)(2,1)}) %all-gather.5.cloned.1.call-update) | async-done | bytes 1572880 | tf_op jit(solution)/shard_map/all_gather | solution.py:62
  50.9 4.2 %fusion.5 = f32[384,704]{0,1:T(8,128)} fusion(bf16[384,2048]{1,0:T(8,128)(2,1)} %bitcast.74, bf16[1,2048,704]{1,2,0:T(8,128)(2,1)S(1)} %copy-done), kind=kOutput, calls=%fused_computation.11 | convolution fusion | flops 1107296256 | bytes 5537792 | tf_op jit(solution)/shard_map/dot_general | solution.py:8
  55.1 2.7 %fusion.9 = f32[384,704]{0,1:T(8,128)} fusion(bf16[384,2048]{1,0:T(8,128)(2,1)S(1)} %bitcast.76, bf16[1,2048,704]{1,2,0:T(8,128)(2,1)S(1)} %copy-done.1), kind=kOutput, calls=%fused_computation.15 | convolution fusion | flops 1107296256 | bytes 5537792 | tf_op jit(solution)/shard_map/dot_general | solution.py:9
  57.8 20.8 %all-gather.3.cloned.1.call-done = bf16[4,96,2048]{2,1,0:T(8,128)(2,1)} async-done(((bf16[4,96,256]{2,1,0:T(8,128)(2,1)}), bf16[4,96,2048]{2,1,0:T(8,128)(2,1)}) %all-gather.3.cloned.1.call-update) | async-done | bytes 1572880 | tf_op jit(solution)/shard_map/all_gather | solution.py:63
  78.6 5.7 %multiply_reduce_fusion = (f32[384]{0:T(512)S(1)}, bf16[384,704]{0,1:T(8,128)(2,1)}, bf16[384,704]{0,1:T(8,128)(2,1)S(1)}, bf16[384,704]{0,1:T(8,128)(2,1)S(1)}) fusion(f32[384,704]{0,1:T(8,128)} %fusion.9, f32[384,704]{0,1:T(8,128)} %fusion.5, bf16[384,2048]{1,0:T(8,128)(2,1)} %bitcast.78, bf16[1,704,2048]{2,1,0:T(8,128)(2,1)} %param.13), kind=kOutput, calls=%fused_computation.23 | convolution fusion | flops 1112161920 | bytes 8242688 | tf_op jit(solution)/shard_map/dot_general | solution.py:12
  84.3 1.4 fusion.3
  86.3 2.6 %add_convert_fusion = bf16[384,2048]{1,0:T(8,128)(2,1)} fusion(f32[384,2048]{1,0:T(8,128)S(1)} %fusion.3, bf16[384,704]{0,1:T(8,128)(2,1)S(1)} %get-tuple-element.23, bf16[1,2048,704]{1,2,0:T(8,128)(2,1)S(1)} %copy-done.2), kind=kOutput, calls=%fused_computation.5 | convolution fusion | flops 1108869120 | bytes 8142848 | tf_op jit(solution)/shard_map/dot_general | solution.py:75
  89.0 1.0 mul.77
  90.0 13.1 %psum.7 = bf16[384]{0:T(512)(128)(2,1)S(1)} all-reduce(f32[384]{0:T(512)S(1)} %get-tuple-element.20), channel_id=1, replica_groups=mesh['ep'=4,'tp'=8] {'tp'}, use_global_device_ids=true, to_apply=%region_7.8 | all-reduce | flops 384 | bytes 2304 | tf_op jit(solution)/shard_map/psum | solution.py:79
  103.1 0.7 convert_element_type.83
  103.8 4.6 %all-to-all-start.3 = ((bf16[4,1,96]{2,1,0:T(2,128)(2,1)}), bf16[4,1,96]{2,1,0:T(2,128)(2,1)S(1)}, u32[]{:S(2)}, u32[]{:S(2)}) async-start(bf16[4,1,96]{2,1,0:T(2,128)(2,1)} %convert_element_type.83), calls=%async_computation.4 | async-start | bytes 4096 | tf_op jit(solution)/shard_map/all_to_all | solution.py:87
  108.4 5.0 %fusion.1 = bf16[1,2048,704]{1,2,0:T(8,128)(2,1)} fusion(bf16[384,704]{0,1:T(8,128)(2,1)S(1)} %get-tuple-element.22, bf16[384,2048]{1,0:T(8,128)(2,1)} %bitcast.75), kind=kOutput, calls=%fused_computation.7 | convolution fusion | flops 1108738048 | bytes 4997120 | tf_op jit(solution)/shard_map/dot_general | solution.py:20
  113.4 3.2 %fusion.2 = bf16[1,2048,704]{1,2,0:T(8,128)(2,1)} fusion(bf16[384,704]{0,1:T(8,128)(2,1)S(1)} %copy-done.4, bf16[384,2048]{1,0:T(8,128)(2,1)S(1)} %bitcast.77), kind=kOutput, calls=%fused_computation.8 | convolution fusion | flops 1108738048 | bytes 4997120 | tf_op jit(solution)/shard_map/dot_general | solution.py:21
  116.7 10.8 %reduce-scatter.2.cloned.1.call-done = bf16[4,96,256]{2,1,0:T(8,128)(2,1)} async-done(((bf16[4,96,2048]{2,1,0:T(8,128)(2,1)}), bf16[4,96,256]{2,1,0:T(8,128)(2,1)}) %reduce-scatter.2.cloned.1.call-update) | async-done | bytes 196624 | tf_op jit(solution)/shard_map/reduce_scatter | solution.py:80
  127.5 4.6 %all-to-all-start.2 = ((bf16[4,96,256]{2,1,0:T(8,128)(2,1)}), bf16[4,96,256]{2,1,0:T(8,128)(2,1)S(1)}, u32[]{:S(2)}, u32[]{:S(2)}) async-start(bf16[4,96,256]{2,1,0:T(8,128)(2,1)} %reduce-scatter.2.cloned.1.call-done), calls=%async_computation.3 | async-start | bytes 393216 | tf_op jit(solution)/shard_map/all_to_all | solution.py:84
  132.1 4.8 %fusion = bf16[1,704,2048]{2,1,0:T(8,128)(2,1)} fusion(bf16[384,704]{0,1:T(8,128)(2,1)} %get-tuple-element.21, bf16[384,2048]{1,0:T(8,128)(2,1)} %bitcast.79), kind=kOutput, calls=%fused_computation.6 | convolution fusion | flops 1108738048 | bytes 4997120 | tf_op jit(solution)/shard_map/dot_general | solution.py:19
  137.0 1.9 %gather_fusion.1 = f32[256]{0:T(256)S(1)} fusion(f32[384]{0:T(512)S(1)} %reshape.139, s32[1024]{0:T(1024)S(1)} %pad_clamp_fusion), kind=kCustom, calls=%fused_computation.1 | custom fusion | bytes 3072 | tf_op jit(solution)/shard_map/gather | solution.py:99
  139.8 1.0 gather_fusion
  140.9 0.9 reduce_sum.34
  (54 shorter events, 4.2 us)
Async XLA Ops:
  7.2 43.7 %copy-start = (bf16[1,2048,704]{1,2,0:T(8,128)(2,1)S(1)}, bf16[1,2048,704]{1,2,0:T(8,128)(2,1)}, u32[]{:S(2)}) copy-start(bf16[1,2048,704]{1,2,0:T(8,128)(2,1)} %param.11) | copy-start | bytes 8650756
  7.2 18.7 %copy-start.6 = (f32[128,2]{0,1:T(2,128)S(1)}, f32[128,2]{0,1:T(2,128)}, u32[]{:S(2)}) copy-start(f32[128,2]{0,1:T(2,128)} %param.10) | copy-start | bytes 3076
  7.2 19.3 %copy-start.5 = (bf16[128,256]{1,0:T(8,128)(2,1)S(1)}, bf16[128,256]{1,0:T(8,128)(2,1)}, u32[]{:S(2)}) copy-start(bf16[128,256]{1,0:T(8,128)(2,1)} %param.8) | copy-start | bytes 196612
  7.2 43.7 %all-gather.5.cloned.1.call-start = ((), (), s32[]{:S(2)}) async-start(), calls=%async_computation.6 | async-start | bytes 1769472 | tf_op jit(solution)/shard_map/all_gather | solution.py:62
  25.8 52.7 %all-gather.3.cloned.1.call-start = ((), (), s32[]{:S(2)}) async-start(), calls=%async_computation.5 | async-start | bytes 1769472 | tf_op jit(solution)/shard_map/all_gather | solution.py:63
  36.6 90.9 %reduce-scatter.2.cloned.1.call-start = ((), (), s32[]{:S(2)}) async-start(), calls=%async_computation.7 | async-start | bytes 1769472 | tf_op jit(solution)/shard_map/reduce_scatter | solution.py:80
  50.9 4.2 %copy-start.1 = (bf16[1,2048,704]{1,2,0:T(8,128)(2,1)S(1)}, bf16[1,2048,704]{1,2,0:T(8,128)(2,1)}, u32[]{:S(2)}) copy-start(bf16[1,2048,704]{1,2,0:T(8,128)(2,1)} %param.12) | copy-start | bytes 8650756
  50.9 4.2 %copy-start.7 = (bf16[4,96,2048]{2,1,0:T(8,128)(2,1)S(1)}, bf16[4,96,2048]{2,1,0:T(8,128)(2,1)}, u32[]{:S(2)}) copy-start(bf16[4,96,2048]{2,1,0:T(8,128)(2,1)} %all-gather.5.cloned.1.call-done) | copy-start | bytes 4718596
  84.3 1.4 copy-start.3
  84.3 2.0 %copy-start.2 = (bf16[1,2048,704]{1,2,0:T(8,128)(2,1)S(1)}, bf16[1,2048,704]{1,2,0:T(8,128)(2,1)}, u32[]{:S(2)}) copy-start(bf16[1,2048,704]{1,2,0:T(8,128)(2,1)} %param.12) | copy-start | bytes 8650756
  103.8 12.9 %all-to-all-start.3 = ((bf16[4,1,96]{2,1,0:T(2,128)(2,1)}), bf16[4,1,96]{2,1,0:T(2,128)(2,1)S(1)}, u32[]{:S(2)}, u32[]{:S(2)}) async-start(bf16[4,1,96]{2,1,0:T(2,128)(2,1)} %convert_element_type.83), calls=%async_computation.4 | async-start | bytes 4096 | tf_op jit(solution)/shard_map/all_to_all | solution.py:87
  108.4 5.0 %copy-start.4 = (bf16[384,704]{0,1:T(8,128)(2,1)S(1)}, bf16[384,704]{0,1:T(8,128)(2,1)}, u32[]{:S(2)}) copy-start(bf16[384,704]{0,1:T(8,128)(2,1)} %copy-done.3) | copy-start | bytes 1622020
  108.4 5.0 %copy-start.8 = (bf16[4,96,2048]{2,1,0:T(8,128)(2,1)S(1)}, bf16[4,96,2048]{2,1,0:T(8,128)(2,1)}, u32[]{:S(2)}) copy-start(bf16[4,96,2048]{2,1,0:T(8,128)(2,1)} %all-gather.5.cloned.1.call-done) | copy-start | bytes 4718596
  127.5 12.3 %all-to-all-start.2 = ((bf16[4,96,256]{2,1,0:T(8,128)(2,1)}), bf16[4,96,256]{2,1,0:T(8,128)(2,1)S(1)}, u32[]{:S(2)}, u32[]{:S(2)}) async-start(bf16[4,96,256]{2,1,0:T(8,128)(2,1)} %reduce-scatter.2.cloned.1.call-done), calls=%async_computation.3 | async-start | bytes 393216 | tf_op jit(solution)/shard_map/all_to_all | solution.py:84
Sparse Core Ops, SparseCore 0:
  26.0 24.8 all-gather.4
  52.8 25.7 all-gather.2
  89.1 38.3 reduce-scatter.1
where the time goes:
time: 149 us; the launch traced here: 148 us
  waiting for transfers between devices  45.9 us (31%)
  blocking collectives  36.7 us (25%)
  matrix products  31.3 us (21%)
  between operations  13.9 us (9%)
  starting transfers between devices  9.33 us (6%)
  local copies, waits for them, and re-layouts  8.1 us (5%)
  other arithmetic  3.1 us (2%)
    all_gather x1, waiting for transfers between devices, on_device(): lax.all_gather(recv_cotan, 'tp', axis=2, tiled=True)  20.8 us
    all_gather x1, waiting for transfers between devices, on_device(): lax.all_gather(recv_rows, 'tp', axis=2, tiled=True)  14.2 us
    all_to_all x1, blocking collectives, on_device(): lax.all_to_all(sent_rows.reshape(ep_size, capacity, slice_width), 'ep', s...  13.7 us
    psum x1, blocking collectives, on_device(): summed = lax.psum(slot_dots, 'tp')  13.1 us
    reduce_scatter x1, waiting for transfers between devices, on_device(): lax.psum_scatter(partial_value.reshape(ep_size, capacity, model_width), '...  10.8 us
    all_to_all x1, blocking collectives, on_device(): lax.all_to_all(sent_cotan.reshape(ep_size, capacity, slice_width), 'ep',...  9.87 us
    dot_general x1, matrix products, expert_grads(): hid_grad = jnp.dot(cotan, w_down.T, preferred_element_type=jnp.float32)  5.73 us
    dot_general x1, matrix products, expert_grads(): jnp.dot(rows.T, gate_part, preferred_element_type=jnp.float32)  5.03 us
  transfers between devices with their start and end apart: 5, of which 3 were waited for; matrix products, arithmetic and copies ran while one was open for 17% of the time, Pallas kernels for 0%

commit v1 on v0

--- a/solution.py
+++ b/solution.py
@@ -60,7 +60,9 @@
     )
     whole_rows, whole_cotan = (
         lax.all_gather(recv_rows, "tp", axis=2, tiled=True),
-        lax.all_gather(recv_cotan, "tp", axis=2, tiled=True),
+        jnp.concatenate(
+            lax.all_to_all(jnp.stack([recv_cotan] * lax.axis_size("tp")), "tp", 0, 0), axis=2
+        ),
     )
     model_width = whole_rows.shape[2]
     rows = whole_rows.reshape(buffer_rows, model_width)

time: 149 us -> 138 us (0.926)
  waiting for transfers between devices: 45.9 us -> 9.52 us
  blocking collectives: 36.7 us -> 64.3 us
  matrix products: 31.3 us -> 26.8 us
  local copies, waits for them, and re-layouts: 8.1 us -> 10.6 us
    all_to_all x0 -> x1, blocking collectives: none -> 28.7 us  [on_device(): lax.all_to_all(jnp.stack([recv_cotan] * lax.axis_size('tp')), 'tp', 0, 0)]
    all_gather x1 -> x0, waiting for transfers between devices: 20.8 us -> none  [on_device(): lax.all_gather(recv_cotan, 'tp', axis=2, tiled=True)]
    all_gather x1, waiting for transfers between devices: 14.2 us -> 0.01 us  [on_device(): lax.all_gather(recv_rows, 'tp', axis=2, tiled=True)]
    dot_general x1, matrix products: 5.73 us -> 3.46 us  [expert_grads(): hid_grad = jnp.dot(cotan, w_down.T, preferred_element_type=jnp.float32)]
    unnamed x21 -> x32, local copies, waits for them, and re-layouts: 2.29 us -> 3.99 us
  transfers between devices with their start and end apart: 5 -> 4, of which waited for: 3 -> 1; matrix products, arithmetic and copies ran while one was open for 17% -> 16% of each run, Pallas kernels for 0% -> 0%
where the time goes in v1:
time: 138 us; the launch traced here: 137 us
  blocking collectives  64.3 us (47%)
  matrix products  26.8 us (19%)
  between operations  14.3 us (10%)
  local copies, waits for them, and re-layouts  10.6 us (8%)
  waiting for transfers between devices  9.52 us (7%)
  starting transfers between devices  8 us (6%)
  other arithmetic  3.76 us (3%)
    all_to_all x1, blocking collectives, on_device(): lax.all_to_all(jnp.stack([recv_cotan] * lax.axis_size('tp')), 'tp', 0, 0)  28.7 us
    all_to_all x1, blocking collectives, on_device(): lax.all_to_all(sent_rows.reshape(ep_size, capacity, slice_width), 'ep', s...  13.7 us
    psum x1, blocking collectives, on_device(): summed = lax.psum(slot_dots, 'tp')  12 us
    all_to_all x1, blocking collectives, on_device(): lax.all_to_all(sent_cotan.reshape(ep_size, capacity, slice_width), 'ep',...  9.94 us
    reduce_scatter x1, waiting for transfers between devices, on_device(): lax.psum_scatter(partial_value.reshape(ep_size, capacity, model_width), '...  9.48 us
    dot_general x1, matrix products, expert_grads(): jnp.dot(hidden.T, cotan, preferred_element_type=jnp.float32)  4.83 us
    dot_general x1, matrix products, expert_grads(): jnp.dot(rows.T, gate_part, preferred_element_type=jnp.float32)  4.79 us
    all_to_all x1, starting transfers between devices, on_device(): lax.all_to_all(row_sums.astype(jnp.bfloat16), 'ep', split_axis=0, concat_...  4.6 us
  transfers between devices with their start and end apart: 4, of which 1 were waited for; matrix products, arithmetic and copies ran while one was open for 16% of the time, Pallas kernels for 0%

profile of v1, /device:TPU:0, one launch (start us, length us, event | category | flops | bytes accessed | tf_op | source)
XLA Modules:
  0.0 137.3 jit_solution(1361706689343082679)
XLA Ops:
  7.2 0.9 copy.33
  8.5 1.2 reduce-window.6
  10.4 1.0 convolution_convert_fusion.3
  11.5 13.7 %all_to_all.26 = bf16[4,96,256]{2,1,0:T(8,128)(2,1)} all-to-all(bf16[4,96,256]{2,1,0:T(8,128)(2,1)S(1)} %bitcast.77), channel_id=1, replica_groups=mesh['ep'=4,'tp'=8] {'ep'}, dimensions={0} | all-to-all | bytes 393216 | tf_op jit(solution)/shard_map/all_to_all | solution.py:46
  26.1 9.9 %all_to_all.27 = bf16[4,96,256]{2,1,0:T(8,128)(2,1)S(1)} all-to-all(bf16[4,96,256]{2,1,0:T(8,128)(2,1)S(1)} %bitcast.76), channel_id=1, replica_groups=mesh['ep'=4,'tp'=8] {'ep'}, dimensions={0} | all-to-all | bytes 393216 | tf_op jit(solution)/shard_map/all_to_all | solution.py:53
  36.2 28.7 %all_to_all.28 = bf16[8,4,96,256]{3,2,1,0:T(8,128)(2,1)S(1)} all-to-all(bf16[8,4,96,256]{3,2,1,0:T(8,128)(2,1)S(1)} %stack.2), channel_id=1, replica_groups=mesh['ep'=4,'tp'=8] {'tp'}, dimensions={0} | all-to-all | bytes 3145728 | tf_op jit(solution)/shard_map/all_to_all | solution.py:64
  64.9 0.9 copy.40
  65.8 1.7 %copy.45 = bf16[48,8,8,256]{3,1,2,0:T(8,128)(2,1)} copy(bf16[48,8,8,256]{3,2,1,0:T(8,128)(2,1)S(1)} %bitcast.72) | data formatting | bytes 3145728
  67.4 3.2 %fusion.5 = f32[384,704]{0,1:T(8,128)S(1)} fusion(bf16[384,2048]{1,0:T(8,128)(2,1)} %bitcast.81, bf16[1,2048,704]{1,2,0:T(8,128)(2,1)S(1)} %copy-done), kind=kOutput, calls=%fused_computation.11 | convolution fusion | flops 1107296256 | bytes 5537792 | tf_op jit(solution)/shard_map/dot_general | solution.py:8
  70.7 1.7 %fusion.9 = f32[384,704]{0,1:T(8,128)S(1)} fusion(bf16[384,2048]{1,0:T(8,128)(2,1)S(1)} %bitcast.83, bf16[1,2048,704]{1,2,0:T(8,128)(2,1)S(1)} %copy-done.1), kind=kOutput, calls=%fused_computation.15 | convolution fusion | flops 1107296256 | bytes 5537792 | tf_op jit(solution)/shard_map/dot_general | solution.py:9
  73.0 3.5 %multiply_reduce_fusion = (f32[384]{0:T(512)}, bf16[384,704]{0,1:T(8,128)(2,1)}, bf16[384,704]{0,1:T(8,128)(2,1)S(1)}, bf16[384,704]{0,1:T(8,128)(2,1)S(1)}) fusion(f32[384,704]{0,1:T(8,128)S(1)} %fusion.9, f32[384,704]{0,1:T(8,128)S(1)} %fusion.5, bf16[384,2048]{1,0:T(8,128)(2,1)S(1)} %bitcast.75, bf16[1,704,2048]{2,1,0:T(8,128)(2,1)S(1)} %copy-done.11), kind=kOutput, calls=%fused_computation.23 | convolution fusion | flops 1112161920 | bytes 8242688 | tf_op jit(solution)/shard_map/dot_general | solution.py:12
  76.4 1.4 %fusion.3 = f32[384,2048]{1,0:T(8,128)S(1)} fusion(bf16[384,704]{0,1:T(8,128)(2,1)S(1)} %get-tuple-element.22, bf16[1,2048,704]{1,2,0:T(8,128)(2,1)S(1)} %copy-done), kind=kOutput, calls=%fused_computation.9 | convolution fusion | flops 1107296256 | bytes 6569984 | tf_op jit(solution)/shard_map/dot_general | solution.py:75
  77.9 2.7 %add_convert_fusion = bf16[384,2048]{1,0:T(8,128)(2,1)} fusion(f32[384,2048]{1,0:T(8,128)S(1)} %fusion.3, bf16[384,704]{0,1:T(8,128)(2,1)S(1)} %get-tuple-element.23, bf16[1,2048,704]{1,2,0:T(8,128)(2,1)S(1)} %copy-done.1), kind=kOutput, calls=%fused_computation.5 | convolution fusion | flops 1108869120 | bytes 8142848 | tf_op jit(solution)/shard_map/dot_general | solution.py:77
  80.6 0.7 mul.77
  82.6 12.0 %psum.7 = bf16[384]{0:T(512)(128)(2,1)S(1)} all-reduce(f32[384]{0:T(512)} %get-tuple-element.20), channel_id=1, replica_groups=mesh['ep'=4,'tp'=8] {'tp'}, use_global_device_ids=true, to_apply=%region_7.8 | all-reduce | flops 384 | bytes 2304 | tf_op jit(solution)/shard_map/psum | solution.py:81
  95.2 3.3 %all-to-all-start.4 = ((bf16[4,1,96]{2,1,0:T(2,128)(2,1)}), bf16[4,1,96]{2,1,0:T(2,128)(2,1)S(1)}, u32[]{:S(2)}, u32[]{:S(2)}) async-start(bf16[4,1,96]{2,1,0:T(2,128)(2,1)} %convert_element_type.83), calls=%async_computation.5 | async-start | bytes 4096 | tf_op jit(solution)/shard_map/all_to_all | solution.py:89
  98.5 4.8 %fusion.1 = bf16[1,2048,704]{1,2,0:T(8,128)(2,1)} fusion(bf16[384,704]{0,1:T(8,128)(2,1)S(1)} %get-tuple-element.22, bf16[384,2048]{1,0:T(8,128)(2,1)} %bitcast.82), kind=kOutput, calls=%fused_computation.7 | convolution fusion | flops 1108738048 | bytes 4997120 | tf_op jit(solution)/shard_map/dot_general | solution.py:20
  103.3 3.2 %fusion.2 = bf16[1,2048,704]{1,2,0:T(8,128)(2,1)} fusion(bf16[384,704]{0,1:T(8,128)(2,1)S(1)} %copy-done.4, bf16[384,2048]{1,0:T(8,128)(2,1)S(1)} %bitcast.84), kind=kOutput, calls=%fused_computation.8 | convolution fusion | flops 1108738048 | bytes 4997120 | tf_op jit(solution)/shard_map/dot_general | solution.py:21
  106.6 9.5 %reduce-scatter.2.cloned.1.call-done = bf16[4,96,256]{2,1,0:T(8,128)(2,1)} async-done(((bf16[4,96,2048]{2,1,0:T(8,128)(2,1)}), bf16[4,96,256]{2,1,0:T(8,128)(2,1)}) %reduce-scatter.2.cloned.1.call-update) | async-done | bytes 196624 | tf_op jit(solution)/shard_map/reduce_scatter | solution.py:82
  116.1 4.6 %all-to-all-start.3 = ((bf16[4,96,256]{2,1,0:T(8,128)(2,1)}), bf16[4,96,256]{2,1,0:T(8,128)(2,1)S(1)}, u32[]{:S(2)}, u32[]{:S(2)}) async-start(bf16[4,96,256]{2,1,0:T(8,128)(2,1)} %reduce-scatter.2.cloned.1.call-done), calls=%async_computation.4 | async-start | bytes 393216 | tf_op jit(solution)/shard_map/all_to_all | solution.py:86
  120.7 4.8 %fusion = bf16[1,704,2048]{2,1,0:T(8,128)(2,1)} fusion(bf16[384,704]{0,1:T(8,128)(2,1)} %get-tuple-element.21, bf16[384,2048]{1,0:T(8,128)(2,1)} %bitcast.74), kind=kOutput, calls=%fused_computation.6 | convolution fusion | flops 1108738048 | bytes 4997120 | tf_op jit(solution)/shard_map/dot_general | solution.py:19
  125.6 1.9 %gather_fusion.1 = f32[256]{0:T(256)S(1)} fusion(f32[384]{0:T(512)S(1)} %reshape.141, s32[1024]{0:T(1024)S(1)} %copy-done.7), kind=kCustom, calls=%fused_computation.1 | custom fusion | bytes 3072 | tf_op jit(solution)/shard_map/gather | solution.py:101
  128.4 1.0 gather_fusion
  129.5 0.9 reduce_sum.34
  (65 shorter events, 5.7 us)
Async XLA Ops:
  7.2 60.3 %copy-start = (bf16[1,2048,704]{1,2,0:T(8,128)(2,1)S(1)}, bf16[1,2048,704]{1,2,0:T(8,128)(2,1)}, u32[]{:S(2)}) copy-start(bf16[1,2048,704]{1,2,0:T(8,128)(2,1)} %param.11) | copy-start | bytes 8650756
  7.2 18.1 %copy-start.10 = (f32[128,2]{0,1:T(2,128)S(1)}, f32[128,2]{0,1:T(2,128)}, u32[]{:S(2)}) copy-start(f32[128,2]{0,1:T(2,128)} %param.10) | copy-start | bytes 3076
  7.2 18.7 %copy-start.5 = (bf16[128,256]{1,0:T(8,128)(2,1)S(1)}, bf16[128,256]{1,0:T(8,128)(2,1)}, u32[]{:S(2)}) copy-start(bf16[128,256]{1,0:T(8,128)(2,1)} %param.8) | copy-start | bytes 196612
  7.2 60.2 %all-gather.2.cloned.1.call-start = ((), (), s32[]{:S(2)}) async-start(), calls=%async_computation.6 | async-start | bytes 1769472 | tf_op jit(solution)/shard_map/all_gather | solution.py:62
  10.1 26.1 %copy-start.6 = (s32[256]{0:T(256)}, s32[256]{0:T(256)S(1)}, u32[]{:S(2)}) copy-start(s32[256]{0:T(256)S(1)} %fusion.21) | copy-start | bytes 3076
  25.2 90.8 %reduce-scatter.2.cloned.1.call-start = ((), (), s32[]{:S(2)}) async-start(), calls=%async_computation.7 | async-start | bytes 1769472 | tf_op jit(solution)/shard_map/reduce_scatter | solution.py:82
  67.4 3.2 %copy-start.1 = (bf16[1,2048,704]{1,2,0:T(8,128)(2,1)S(1)}, bf16[1,2048,704]{1,2,0:T(8,128)(2,1)}, u32[]{:S(2)}) copy-start(bf16[1,2048,704]{1,2,0:T(8,128)(2,1)} %param.12) | copy-start | bytes 8650756
  67.4 3.2 %copy-start.12 = (bf16[4,96,2048]{2,1,0:T(8,128)(2,1)S(1)}, bf16[4,96,2048]{2,1,0:T(8,128)(2,1)}, u32[]{:S(2)}) copy-start(bf16[4,96,2048]{2,1,0:T(8,128)(2,1)} %all-gather.2.cloned.1.call-done) | copy-start | bytes 4718596
  70.7 1.7 %copy-start.2 = (bf16[48,8,8,256]{3,1,2,0:T(8,128)(2,1)S(1)}, bf16[48,8,8,256]{3,1,2,0:T(8,128)(2,1)}, u32[]{:S(2)}) copy-start(bf16[48,8,8,256]{3,1,2,0:T(8,128)(2,1)} %copy.45) | copy-start | bytes 4718596
  70.7 2.3 %copy-start.11 = (bf16[1,704,2048]{2,1,0:T(8,128)(2,1)S(1)}, bf16[1,704,2048]{2,1,0:T(8,128)(2,1)}, u32[]{:S(2)}) copy-start(bf16[1,704,2048]{2,1,0:T(8,128)(2,1)} %param.13) | copy-start | bytes 8650756
  76.4 1.4 %copy-start.3 = (bf16[384,704]{0,1:T(8,128)(2,1)}, bf16[384,704]{0,1:T(8,128)(2,1)S(1)}, u32[]{:S(2)}) copy-start(bf16[384,704]{0,1:T(8,128)(2,1)S(1)} %get-tuple-element.23) | copy-start | bytes 1622020
  95.2 11.4 %all-to-all-start.4 = ((bf16[4,1,96]{2,1,0:T(2,128)(2,1)}), bf16[4,1,96]{2,1,0:T(2,128)(2,1)S(1)}, u32[]{:S(2)}, u32[]{:S(2)}) async-start(bf16[4,1,96]{2,1,0:T(2,128)(2,1)} %convert_element_type.83), calls=%async_computation.5 | async-start | bytes 4096 | tf_op jit(solution)/shard_map/all_to_all | solution.py:89
  98.5 4.8 %copy-start.4 = (bf16[384,704]{0,1:T(8,128)(2,1)S(1)}, bf16[384,704]{0,1:T(8,128)(2,1)}, u32[]{:S(2)}) copy-start(bf16[384,704]{0,1:T(8,128)(2,1)} %copy-done.3) | copy-start | bytes 1622020
  98.5 4.8 %copy-start.13 = (bf16[4,96,2048]{2,1,0:T(8,128)(2,1)S(1)}, bf16[4,96,2048]{2,1,0:T(8,128)(2,1)}, u32[]{:S(2)}) copy-start(bf16[4,96,2048]{2,1,0:T(8,128)(2,1)} %all-gather.2.cloned.1.call-done) | copy-start | bytes 4718596
  106.6 9.5 %copy-start.8 = (bf16[4,1,96]{2,1,0:T(2,128)(2,1)}, bf16[4,1,96]{2,1,0:T(2,128)(2,1)S(1)}, u32[]{:S(2)}) copy-start(bf16[4,1,96]{2,1,0:T(2,128)(2,1)S(1)} %all-to-all-done.4) | copy-start | bytes 2308
  116.1 12.3 %all-to-all-start.3 = ((bf16[4,96,256]{2,1,0:T(8,128)(2,1)}), bf16[4,96,256]{2,1,0:T(8,128)(2,1)S(1)}, u32[]{:S(2)}, u32[]{:S(2)}) async-start(bf16[4,96,256]{2,1,0:T(8,128)(2,1)} %reduce-scatter.2.cloned.1.call-done), calls=%async_computation.4 | async-start | bytes 393216 | tf_op jit(solution)/shard_map/all_to_all | solution.py:86
  120.7 4.8 %copy-start.9 = (bf16[4,1,96]{2,1,0:T(2,128)(2,1)S(1)}, bf16[4,1,96]{2,1,0:T(2,128)(2,1)}, u32[]{:S(2)}) copy-start(bf16[4,1,96]{2,1,0:T(2,128)(2,1)} %copy-done.8) | copy-start | bytes 2308
  120.7 4.9 %copy-start.7 = (s32[1024]{0:T(1024)S(1)}, s32[1024]{0:T(1024)}, u32[]{:S(2)}) copy-start(s32[1024]{0:T(1024)} %pad_clamp_fusion) | copy-start | bytes 12292
Sparse Core Ops, SparseCore 0:
  25.3 33.0 all-gather.1
  80.7 35.3 reduce-scatter.1
